TPU v7x, 32 devices: a whole 2x2x4 slice. The times are simulated.
32 devices in a mesh: sp: 8 (over z, y), tp: 4 (over x, core).
Axes of the slice: x: 2, y: 2, z: 4, core: 2. Of those that a mesh axis runs over, the one named last changes fastest.
Arguments:
- resid: bfloat16 [4096, 2048], P('sp', 'tp'), may hold values from -41 to 41
- queries: bfloat16 [4096, 1024], P('sp', 'tp'), may hold values from -6 to 6
- keys: bfloat16 [4096, 1024], P('sp', 'tp'), may hold values from -6 to 6
- values: bfloat16 [4096, 1024], P('sp', 'tp'), may hold values from -6 to 6
- mix_lambda: float32 [8], P('tp'), may hold values from 0.3 to 0.8
- head_gain: float32 [128], replicated, may hold values from 0.1 to 1.9
- out_weight: bfloat16 [1024, 2048], P(None, 'tp'), may hold values from -0.1875 to 0.1875
- norm_gain: float32 [2048], P('tp'), may hold values from 0.1 to 1.9
- gate_weight: bfloat16 [2048, 5632], P('sp', 'tp'), may hold values from -0.125 to 0.125
- up_weight: bfloat16 [2048, 5632], P('sp', 'tp'), may hold values from -0.125 to 0.125
- conv_weight: float32 [3, 5632], P(None, 'tp'), may hold values from -3.5 to 3.5
- conv_bias: float32 [5632], P('tp'), may hold values from -3 to 3
- down_weight: bfloat16 [5632, 2048], P('tp', 'sp'), may hold values from -0.078125 to 0.078125
Outputs:
- layer_out: bfloat16 [4096, 2048], P('sp', 'tp')
All inputs are finite; a program needn't handle non-finite values.
Results may differ from a plain program's by a relative error of at most 0.009.
Values may be sent and summed in bfloat16 or wider, within the bound.
A program may use at most 128 MiB of HBM per device.

v0:
```python
import math
import jax
import jax.numpy as jnp
from jax import lax
from jax.sharding import PartitionSpec as P

D = 2048
HD = 64
VD = 128


def with_halo(cells, sides, width):
    for axis, dim in sides:
        count = lax.axis_size(axis)
        ends = count - 1
        head = lax.slice_in_dim(cells, 0, width, axis=dim)
        tail = lax.slice_in_dim(cells, cells.shape[dim] - width, cells.shape[dim], axis=dim)
        cells = jnp.concatenate(
            [
                lax.ppermute(tail, axis, [(i, (i + 1) % count) for i in range(ends)]),
                cells,
                lax.ppermute(head, axis, [((i + 1) % count, i) for i in range(ends)]),
            ],
            axis=dim,
        )
    return cells


def on_device(
    resid,
    queries,
    keys,
    values,
    mix_lambda,
    head_gain,
    out_weight,
    norm_gain,
    gate_weight,
    up_weight,
    conv_weight,
    conv_bias,
    down_weight,
):
    length = queries.shape[0]
    heads = mix_lambda.shape[0]
    scale = HD ** (-0.5)
    query_heads = queries.reshape(length, heads, 2, HD)
    initial = (
        jnp.full((heads, 2, length), -1e30, jnp.float32),
        jnp.zeros((heads, 2, length), jnp.float32),
        jnp.zeros((heads, 2, length, VD), jnp.float32),
    )
    key_rows = lax.all_gather(keys, "sp", axis=0, tiled=True)
    value_rows = lax.all_gather(values, "sp", axis=0, tiled=True)
    count = key_rows.shape[0]
    block = math.gcd(count, 2048)
    key_blocks = key_rows.reshape(count // block, block, heads, 2, HD)
    value_blocks = value_rows.reshape(count // block, block, heads, VD)

    def advance(state, blocks):
        running, totals, weighted = state
        key_block, value_block = blocks
        scores = (
            jnp.einsum(
                "qhmd,khmd->hmqk", query_heads, key_block, preferred_element_type=jnp.float32
            )
            * scale
        )
        highest = jnp.maximum(running, jnp.max(scores, axis=-1))
        factor = jnp.exp(running - highest)
        shifted = jnp.exp(scores - highest[..., None])
        totals = totals * factor + jnp.sum(shifted, axis=-1)
        weighted = weighted * factor[..., None] + jnp.einsum(
            "hmqk,khe->hmqe",
            shifted.astype(jnp.bfloat16),
            value_block,
            preferred_element_type=jnp.float32,
        )
        return ((highest, totals, weighted), None)

    result, unused = lax.scan(advance, initial, (key_blocks, value_blocks))
    running, totals, weighted = result
    mapped = weighted / totals[..., None]
    mixed = mapped[:, 0] - mix_lambda[:, None, None] * mapped[:, 1]
    spread = jnp.mean(mixed * mixed, axis=-1, keepdims=True)
    normed = mixed * lax.rsqrt(spread + 1e-06) * head_gain * 0.8
    heads_out = jnp.transpose(normed, (1, 0, 2)).reshape(length, heads * VD).astype(jnp.bfloat16)
    projected = jnp.dot(
        lax.all_gather(heads_out, "tp", axis=1, tiled=True),
        out_weight,
        preferred_element_type=jnp.float32,
    )
    after_mixer = resid.astype(jnp.float32) + projected
    squares = lax.psum(jnp.sum(after_mixer * after_mixer, axis=1), "tp")
    normed_rows = (after_mixer * lax.rsqrt(squares / D + 1e-06)[:, None] * norm_gain).astype(
        jnp.bfloat16
    )
    full_rows = lax.all_gather(normed_rows, "tp", axis=1, tiled=True)
    gate_sum = jnp.dot(
        full_rows,
        lax.all_gather(gate_weight, "sp", axis=0, tiled=True),
        preferred_element_type=jnp.float32,
    )
    upward = jnp.dot(
        full_rows,
        lax.all_gather(up_weight, "sp", axis=0, tiled=True),
        preferred_element_type=jnp.float32,
    )
    gated = gate_sum.astype(jnp.bfloat16)
    padded = with_halo(gated, (("sp", 0),), 1).astype(jnp.float32)
    conv = (
        padded[:-2] * conv_weight[0]
        + padded[1:-1] * conv_weight[1]
        + padded[2:] * conv_weight[2]
        + conv_bias
    )
    hidden = (jax.nn.silu(conv) * upward).astype(jnp.bfloat16)
    partial_terms = jnp.dot(
        hidden,
        lax.all_gather(down_weight, "sp", axis=1, tiled=True),
        preferred_element_type=jnp.float32,
    )
    mixer_out = lax.psum_scatter(
        partial_terms.astype(jnp.bfloat16), "tp", scatter_dimension=1, tiled=True
    ).astype(jnp.float32)
    return (after_mixer + mixer_out).astype(jnp.bfloat16)


def solution(mesh):
    placed = (
        P("sp", "tp"),
        P("sp", "tp"),
        P("sp", "tp"),
        P("sp", "tp"),
        P("tp"),
        P(),
        P(None, "tp"),
        P("tp"),
        P("sp", "tp"),
        P("sp", "tp"),
        P(None, "tp"),
        P("tp"),
        P("tp", "sp"),
    )
    return jax.shard_map(
        on_device, mesh=mesh, in_specs=placed, out_specs=P("sp", "tp"), check_vma=False
    )
```

profile of v0, /device:TPU:0, one launch (start us, length us, event | category | flops | bytes accessed | tf_op | source)
XLA Modules:
  0.0 553.9 jit_solution(7031731348143616948)
XLA Ops:
  8.1 1.1 copy.23
  9.2 52.1 %all-gather.8.cloned.1.call-done = bf16[4096,256]{1,0:T(8,128)(2,1)} async-done(((bf16[512,256]{1,0:T(8,128)(2,1)}), bf16[4096,256]{1,0:T(8,128)(2,1)}) %all-gather.8.cloned.1.call-update) | async-done | bytes 2097168 | tf_op jit(solution)/shard_map/all_gather | solution.py:53
  61.3 8.3 %reshape.31 = bf16[2,2048,2,2,64]{4,3,2,1,0:T(2,128)(2,1)} reshape(bf16[4096,256]{1,0:T(8,128)(2,1)} %all-gather.8.cloned.1.call-done) | data formatting | bytes 4194304 | tf_op jit(solution)/shard_map/reshape | solution.py:57
  69.6 10.7 %copy.24 = bf16[2,2048,2,2,64]{1,4,3,2,0:T(8,128)(2,1)} copy(bf16[2,2048,2,2,64]{4,3,2,1,0:T(2,128)(2,1)} %reshape.31) | data formatting | bytes 4194304
  80.3 30.7 %all-gather.10.cloned.1.call-done = bf16[4096,256]{1,0:T(8,128)(2,1)} async-done(((bf16[512,256]{1,0:T(8,128)(2,1)}), bf16[4096,256]{1,0:T(8,128)(2,1)}) %all-gather.10.cloned.1.call-update) | async-done | bytes 2097168 | tf_op jit(solution)/shard_map/all_gather | solution.py:54
  111.1 4.0 reshape.29
  115.0 53.5 %while.15 = (s32[]{:T(128)}, f32[2,2,512]{2,1,0:T(2,128)S(1)}, f32[2,2,512]{2,1,0:T(2,128)S(1)}, f32[2,2,512,128]{3,2,1,0:T(8,128)S(1)}, bf16[2,2048,2,2,64]{1,4...) while((s32[]{:T(128)}, f32[2,2,512]{2,1,0:T(2,128)S(1)}, ...), condition=%wide.region_3.4_spmd.clone, body=%wide.region_0.3_spmd.clone.sunk | while | flops 1644963840 | bytes 65405572 | solution.py:81
  115.0 9.3 %bitcast_reduce_fusion.2 = (f32[2,2,512]{2,1,0:T(2,128)S(1)}, f32[2,2,2048,512]{3,2,1,0:T(8,128)}) fusion(bf16[512,2,2,64]{0,3,2,1:T(8,128)(2,1)S(1)} %get-tuple-element.175, bf16[2,2048,2,2,64]{1,4,3,2,0:T(8,128)(2,1)} %get-tuple-element.174, s32[]{:T(128)} %get-tuple-element.161), kind=kOutput, calls=%fused_computation.1.clone.1 | convolution fusion | flops 545257472 | bytes 18096640 | tf_op jit(solution)/shard_map/while/body/eval_jaxpr/qhmd,khmd->hmqk/dot_general | solution.py:64
  124.4 8.6 %fusion.40 = f32[2,2,512]{2,1,0:T(2,128)S(1)} fusion(f32[2,2,2048,512]{3,2,1,0:T(8,128)} %get-tuple-element.149, f32[2,2,512]{2,1,0:T(2,128)S(1)} %fusion.39), kind=kLoop, calls=%fused_computation.4.clone.1 | loop fusion | flops 12580864 | bytes 16793600 | tf_op jit(solution)/shard_map/while/body/eval_jaxpr/reduce_sum | solution.py:72
  133.1 0.8 constant_dynamic-slice_fusion.2
  133.9 7.9 %fusion.42 = f32[2,2,512,128]{3,2,1,0:T(8,128)S(1)} fusion(f32[2,2,2048,512]{3,2,1,0:T(8,128)} %get-tuple-element.149, f32[2,2,512]{2,1,0:T(2,128)S(1)} %fusion.39, bf16[1,2048,2,128]{3,2,1,0:T(2,128)(2,1)S(1)} %constant_dynamic-slice_fusion.2, f32[2,2,512,128]{3,2,1,0:T(8,128)S(1)} %get-tuple-element.164, f32[2,2,512]{2,1,0:T(2,128)S(1)} %get-tuple-element.151, ...), kind=kOutput, calls=%fused_computation.6.clone.1 | convolution fusion | flops 1087111168 | bytes 19939328 | tf_op jit(solution)/shard_map/while/body/eval_jaxpr/hmqk,khe->hmqe/dot_general | solution.py:73
  141.8 9.3 %bitcast_reduce_fusion.2 = (f32[2,2,512]{2,1,0:T(2,128)S(1)}, f32[2,2,2048,512]{3,2,1,0:T(8,128)}) fusion(bf16[512,2,2,64]{0,3,2,1:T(8,128)(2,1)S(1)} %get-tuple-element.175, bf16[2,2048,2,2,64]{1,4,3,2,0:T(8,128)(2,1)} %get-tuple-element.174, s32[]{:T(128)} %get-tuple-element.161), kind=kOutput, calls=%fused_computation.1.clone.1 | convolution fusion | flops 545257472 | bytes 18096640 | tf_op jit(solution)/shard_map/while/body/eval_jaxpr/qhmd,khmd->hmqk/dot_general | solution.py:64
  151.2 8.6 %fusion.40 = f32[2,2,512]{2,1,0:T(2,128)S(1)} fusion(f32[2,2,2048,512]{3,2,1,0:T(8,128)} %get-tuple-element.149, f32[2,2,512]{2,1,0:T(2,128)S(1)} %fusion.39), kind=kLoop, calls=%fused_computation.4.clone.1 | loop fusion | flops 12580864 | bytes 16793600 | tf_op jit(solution)/shard_map/while/body/eval_jaxpr/reduce_sum | solution.py:72
  160.6 7.9 %fusion.42 = f32[2,2,512,128]{3,2,1,0:T(8,128)S(1)} fusion(f32[2,2,2048,512]{3,2,1,0:T(8,128)} %get-tuple-element.149, f32[2,2,512]{2,1,0:T(2,128)S(1)} %fusion.39, bf16[1,2048,2,128]{3,2,1,0:T(2,128)(2,1)S(1)} %constant_dynamic-slice_fusion.2, f32[2,2,512,128]{3,2,1,0:T(8,128)S(1)} %get-tuple-element.164, f32[2,2,512]{2,1,0:T(2,128)S(1)} %get-tuple-element.151, ...), kind=kOutput, calls=%fused_computation.6.clone.1 | convolution fusion | flops 1087111168 | bytes 19939328 | tf_op jit(solution)/shard_map/while/body/eval_jaxpr/hmqk,khe->hmqe/dot_general | solution.py:73
  169.4 0.9 multiply_convert_fusion.1
  170.8 14.9 %all-gather.12.cloned.1.call-done = bf16[512,1024]{0,1:T(8,128)(2,1)} async-done(((bf16[512,256]{0,1:T(8,128)(2,1)}), bf16[512,1024]{0,1:T(8,128)(2,1)}) %all-gather.12.cloned.1.call-update) | async-done | bytes 1048592 | tf_op jit(solution)/shard_map/all_gather | solution.py:89
  185.7 2.0 multiply_reduce_fusion
  187.7 5.9 %psum.7 = f32[512]{0:T(512)S(1)} all-reduce(f32[512]{0:T(512)S(1)} %get-tuple-element.99), channel_id=1, replica_groups=mesh['sp'=8,'tp'=4] {'tp'}, use_global_device_ids=true, to_apply=%region_6.7 | all-reduce | flops 512 | bytes 4096 | tf_op jit(solution)/shard_map/psum | solution.py:94
  193.6 0.9 multiply_convert_fusion
  196.5 21.8 %all-gather.14.cloned.1.call-done = bf16[512,2048]{0,1:T(8,128)(2,1)} async-done(((bf16[512,512]{0,1:T(8,128)(2,1)}), bf16[512,2048]{0,1:T(8,128)(2,1)}) %all-gather.14.cloned.1.call-update) | async-done | bytes 2097168 | tf_op jit(solution)/shard_map/all_gather | solution.py:98
  218.3 94.4 %all-gather.16.cloned.1.call-done = bf16[2048,1408]{1,0:T(8,128)(2,1)} async-done(((bf16[256,1408]{1,0:T(8,128)(2,1)}), bf16[2048,1408]{1,0:T(8,128)(2,1)}) %all-gather.16.cloned.1.call-update) | async-done | bytes 5767184 | tf_op jit(solution)/shard_map/all_gather | solution.py:101
  312.7 6.7 %convolution_convert_fusion = bf16[512,1408]{1,0:T(8,128)(2,1)S(1)} fusion(bf16[512,2048]{0,1:T(8,128)(2,1)} %all-gather.14.cloned.1.call-done, bf16[2048,1408]{1,0:T(8,128)(2,1)} %all-gather.16.cloned.1.call-done), kind=kOutput, calls=%fused_computation.22 | convolution fusion | flops 2953510912 | bytes 9306112 | tf_op jit(solution)/shard_map/dot_general | solution.py:99
  319.5 2.5 collective-permute-start
  321.9 1.3 collective-permute-start.1
  323.3 4.4 collective-permute-done.1
  327.7 2.0 maximum_convert_fusion
  329.7 75.6 %all-gather.18.cloned.1.call-done = bf16[2048,1408]{1,0:T(8,128)(2,1)} async-done(((bf16[256,1408]{1,0:T(8,128)(2,1)}), bf16[2048,1408]{1,0:T(8,128)(2,1)}) %all-gather.18.cloned.1.call-update) | async-done | bytes 5767184 | tf_op jit(solution)/shard_map/all_gather | solution.py:106
  405.3 93.4 %all-gather.20.cloned.1.call-done = bf16[1408,2048]{1,0:T(8,128)(2,1)} async-done(((bf16[1408,256]{1,0:T(8,128)(2,1)}), bf16[1408,2048]{1,0:T(8,128)(2,1)}) %all-gather.20.cloned.1.call-update) | async-done | bytes 5767184 | tf_op jit(solution)/shard_map/all_gather | solution.py:120
  498.7 16.7 %convolution_convert_fusion.1 = bf16[512,2048]{0,1:T(8,128)(2,1)} fusion(bf16[1408,2048]{1,0:T(8,128)(2,1)} %all-gather.20.cloned.1.call-done, bf16[512,2048]{0,1:T(8,128)(2,1)} %all-gather.14.cloned.1.call-done, bf16[2048,1408]{1,0:T(8,128)(2,1)} %all-gather.18.cloned.1.call-done, f32[514,1408]{1,0:T(8,128)} %maximum_convert_fusion, ...), kind=kOutput, calls=%fused_computation.23 | convolution fusion | flops 5915279360 | bytes 24401920 | tf_op jit(solution)/shard_map/dot_general | solution.py:118
  515.4 29.5 %reduce-scatter.2.cloned.1.call-done = bf16[512,512]{0,1:T(8,128)(2,1)} async-done(((bf16[512,2048]{0,1:T(8,128)(2,1)}), bf16[512,512]{0,1:T(8,128)(2,1)}) %reduce-scatter.2.cloned.1.call-update) | async-done | bytes 524304 | tf_op jit(solution)/shard_map/reduce_scatter | solution.py:123
  544.9 1.2 add_convert_fusion
  546.1 1.0 copy.29
  (54 shorter events, 5.6 us)
Async XLA Ops:
  6.5 179.2 %copy-start = (bf16[1024,512]{1,0:T(8,128)(2,1)S(1)}, bf16[1024,512]{1,0:T(8,128)(2,1)}, u32[]{:S(2)}) copy-start(bf16[1024,512]{1,0:T(8,128)(2,1)} %param.21) | copy-start | bytes 3145732
  6.5 54.8 %all-gather.8.cloned.1.call-start = ((), (), s32[]{:S(2)}) async-start(), calls=%async_computation.1 | async-start | bytes 2359296 | tf_op jit(solution)/shard_map/all_gather | solution.py:53
  7.3 103.8 %all-gather.10.cloned.1.call-start = ((), (), s32[]{:S(2)}) async-start(), calls=%async_computation.2 | async-start | bytes 2359296 | tf_op jit(solution)/shard_map/all_gather | solution.py:54
  8.0 177.7 %all-gather.12.cloned.1.call-start = ((), (), s32[]{:S(2)}) async-start(), calls=%async_computation.3 | async-start | bytes 1310720 | tf_op jit(solution)/shard_map/all_gather | solution.py:89
  124.4 8.7 %copy-start.1 = (bf16[2,2048,2,128]{3,2,1,0:T(2,128)(2,1)S(1)}, bf16[2,2048,2,128]{3,2,1,0:T(2,128)(2,1)}, u32[]{:S(2)}) copy-start(bf16[2,2048,2,128]{3,2,1,0:T(2,128)(2,1)} %get-tuple-element.176) | copy-start | bytes 6291460 | tf_op jit(solution)/shard_map/while
  151.1 8.7 %copy-start.1 = (bf16[2,2048,2,128]{3,2,1,0:T(2,128)(2,1)S(1)}, bf16[2,2048,2,128]{3,2,1,0:T(2,128)(2,1)}, u32[]{:S(2)}) copy-start(bf16[2,2048,2,128]{3,2,1,0:T(2,128)(2,1)} %get-tuple-element.176) | copy-start | bytes 6291460 | tf_op jit(solution)/shard_map/while
  168.5 0.7 copy-start.5
  168.6 0.8 copy-start.6
  168.9 1.6 copy-start.2
  170.3 48.0 %all-gather.14.cloned.1.call-start = ((), (), s32[]{:S(2)}) async-start(), calls=%async_computation.4 | async-start | bytes 2621440 | tf_op jit(solution)/shard_map/all_gather | solution.py:98
  170.8 22.8 %copy-start.4 = (f32[512]{0:T(512)S(1)}, f32[512]{0:T(512)}, u32[]{:S(2)}) copy-start(f32[512]{0:T(512)} %param.22) | copy-start | bytes 6148
  194.6 118.2 %all-gather.16.cloned.1.call-start = ((), (), s32[]{:S(2)}) async-start(), calls=%async_computation.5 | async-start | bytes 6488064 | tf_op jit(solution)/shard_map/all_gather | solution.py:101
  195.1 210.1 %all-gather.18.cloned.1.call-start = ((), (), s32[]{:S(2)}) async-start(), calls=%async_computation.6 | async-start | bytes 6488064 | tf_op jit(solution)/shard_map/all_gather | solution.py:106
  195.7 302.9 %all-gather.20.cloned.1.call-start = ((), (), s32[]{:S(2)}) async-start(), calls=%async_computation.7 | async-start | bytes 6488064 | tf_op jit(solution)/shard_map/all_gather | solution.py:120
  196.5 126.8 %copy-start.3 = (f32[3,1408]{1,0:T(4,128)S(1)}, f32[3,1408]{1,0:T(4,128)}, u32[]{:S(2)}) copy-start(f32[3,1408]{1,0:T(4,128)} %param.25) | copy-start | bytes 50692
  196.5 348.4 %reduce-scatter.2.cloned.1.call-start = ((), (), s32[]{:S(2)}) async-start(), calls=%async_computation.8 | async-start | bytes 2621440 | tf_op jit(solution)/shard_map/reduce_scatter | solution.py:123
  319.4 179.2 %copy-start.7 = (f32[1408]{0:T(1024)S(1)}, f32[1408]{0:T(1024)}, u32[]{:S(2)}) copy-start(f32[1408]{0:T(1024)} %param.26) | copy-start | bytes 16900
  319.5 3.8 collective-permute-start
  321.9 5.8 %collective-permute-start.1 = (bf16[1,1408]{1,0:T(2,128)(2,1)S(1)}, bf16[1,1408]{1,0:T(2,128)(2,1)S(1)}, u32[]{:S(2)}, u32[]{:S(2)}) collective-permute-start(bf16[1,1408]{1,0:T(2,128)(2,1)S(1)} %get-tuple-element.98), channel_id=1, source_target_pairs={{4,0},{8,4},{12,8},{16,12},{20,16},{24,20},{28,24},{5,1},{9,5},{13... | collective-permute-start | bytes 8456 | tf_op jit(solution)/shard_map/ppermute | solution.py:22
Sparse Core Ops, SparseCore 0:
  9.5 51.7 all-gather.7
  63.4 47.6 all-gather.9
  170.4 15.2 all-gather.11
  194.7 23.6 all-gather.13
  220.4 92.3 all-gather.15
  314.7 90.4 all-gather.17
  407.3 91.2 all-gather.19
  515.5 29.3 reduce-scatter.1
where the time goes:
time: 555 us; the launch traced here: 554 us
  waiting for transfers between devices  420 us (76%)
  matrix products  59.9 us (11%)
  local copies, waits for them, and re-layouts  27.4 us (5%)
  other arithmetic  22.7 us (4%)
  between operations  13.7 us (2%)
  blocking collectives  5.88 us (1%)
    all_gather x1, waiting for transfers between devices, on_device(): lax.all_gather(gate_weight, 'sp', axis=0, tiled=True)  94.4 us
    all_gather x1, waiting for transfers between devices, on_device(): lax.all_gather(down_weight, 'sp', axis=1, tiled=True)  93.4 us
    all_gather x1, waiting for transfers between devices, on_device(): lax.all_gather(up_weight, 'sp', axis=0, tiled=True)  75.6 us
    all_gather x1, waiting for transfers between devices, on_device(): key_rows = lax.all_gather(keys, 'sp', axis=0, tiled=True)  52.1 us
    all_gather x1, waiting for transfers between devices, on_device(): value_rows = lax.all_gather(values, 'sp', axis=0, tiled=True)  30.7 us
    reduce_scatter x1, waiting for transfers between devices, on_device(): lax.psum_scatter(partial_terms.astype(jnp.bfloat16), 'tp', scatter_dimens...  29.5 us
    all_gather x1, waiting for transfers between devices, on_device(): full_rows = lax.all_gather(normed_rows, 'tp', axis=1, tiled=True)  21.8 us
    dot_general x2, matrix products, advance(): jnp.einsum('qhmd,khmd->hmqk', query_heads, key_block, preferred_element_t...  18.7 us
  transfers between devices with their start and end apart: 10, of which 9 were waited for; matrix products, arithmetic and copies ran while one was open for 5% of the time, Pallas kernels for 0%

commit v1 on v0

--- a/solution.py
+++ b/solution.py
@@ -115,10 +115,12 @@
         + conv_bias
     )
     hidden = (jax.nn.silu(conv) * upward).astype(jnp.bfloat16)
+
+    def turn_spot_on_mesh(z, row_axis, dim_no=1):
+        return jnp.concatenate(jax.lax.all_gather(z, axis_name=row_axis), axis=dim_no)
+
     partial_terms = jnp.dot(
-        hidden,
-        lax.all_gather(down_weight, "sp", axis=1, tiled=True),
-        preferred_element_type=jnp.float32,
+        hidden, turn_spot_on_mesh(down_weight, "sp"), preferred_element_type=jnp.float32
     )
     mixer_out = lax.psum_scatter(
         partial_terms.astype(jnp.bfloat16), "tp", scatter_dimension=1, tiled=True

time: 555 us -> 554 us (level)
  waiting for transfers between devices: 420 us -> 408 us
  local copies, waits for them, and re-layouts: 27.4 us -> 37.7 us
    all_gather x1, waiting for transfers between devices: 93.4 us -> 79.5 us  [turn_spot_on_mesh(): jax.lax.all_gather(z, axis_name=row_axis)]
    reshape x0 -> x1, local copies, waits for them, and re-layouts: none -> 8.29 us  [turn_spot_on_mesh(): jnp.concatenate(jax.lax.all_gather(z, axis_name=row_axis), axis=dim_no)]
    all_gather x1, waiting for transfers between devices: 75.6 us -> 81.7 us  [on_device(): lax.all_gather(up_weight, 'sp', axis=0, tiled=True)]
    unnamed x17 -> x13, local copies, waits for them, and re-layouts: 12.2 us -> 12.1 us
  transfers between devices with their start and end apart: 10 -> 10, of which waited for: 9 -> 8; matrix products, arithmetic and copies ran while one was open for 5% -> 7% of each run, Pallas kernels for 0% -> 0%
where the time goes in v1:
time: 554 us; the launch traced here: 553 us
  waiting for transfers between devices  408 us (74%)
  matrix products  59.7 us (11%)
  local copies, waits for them, and re-layouts  37.7 us (7%)
  other arithmetic  23.4 us (4%)
  between operations  13.6 us (2%)
  blocking collectives  5.88 us (1%)
    all_gather x1, waiting for transfers between devices, on_device(): lax.all_gather(gate_weight, 'sp', axis=0, tiled=True)  94.4 us
    all_gather x1, waiting for transfers between devices, on_device(): lax.all_gather(up_weight, 'sp', axis=0, tiled=True)  81.7 us
    all_gather x1, waiting for transfers between devices, turn_spot_on_mesh(): jax.lax.all_gather(z, axis_name=row_axis)  79.5 us
    all_gather x1, waiting for transfers between devices, on_device(): key_rows = lax.all_gather(keys, 'sp', axis=0, tiled=True)  52.1 us
    all_gather x1, waiting for transfers between devices, on_device(): value_rows = lax.all_gather(values, 'sp', axis=0, tiled=True)  30.8 us
    reduce_scatter x1, waiting for transfers between devices, on_device(): lax.psum_scatter(partial_terms.astype(jnp.bfloat16), 'tp', scatter_dimens...  29.5 us
    all_gather x1, waiting for transfers between devices, on_device(): full_rows = lax.all_gather(normed_rows, 'tp', axis=1, tiled=True)  21.8 us
    dot_general x2, matrix products, advance(): jnp.einsum('qhmd,khmd->hmqk', query_heads, key_block, preferred_element_t...  18.7 us
  transfers between devices with their start and end apart: 10, of which 8 were waited for; matrix products, arithmetic and copies ran while one was open for 7% of the time, Pallas kernels for 0%

profile of v1, /device:TPU:0, one launch (start us, length us, event | category | flops | bytes accessed | tf_op | source)
XLA Modules:
  0.0 553.1 jit_solution(7220179585889094106)
XLA Ops:
  8.1 1.1 copy.33
  9.2 52.1 %all-gather.9.cloned.1.call-done = bf16[4096,256]{1,0:T(8,128)(2,1)} async-done(((bf16[512,256]{1,0:T(8,128)(2,1)}), bf16[4096,256]{1,0:T(8,128)(2,1)}) %all-gather.9.cloned.1.call-update) | async-done | bytes 2097168 | tf_op jit(solution)/shard_map/all_gather | solution.py:53
  61.3 8.3 %reshape.40 = bf16[2,2048,2,2,64]{4,3,2,1,0:T(2,128)(2,1)} reshape(bf16[4096,256]{1,0:T(8,128)(2,1)} %all-gather.9.cloned.1.call-done) | data formatting | bytes 4194304 | tf_op jit(solution)/shard_map/reshape | solution.py:57
  69.6 10.7 %copy.34 = bf16[2,2048,2,2,64]{1,4,3,2,0:T(8,128)(2,1)} copy(bf16[2,2048,2,2,64]{4,3,2,1,0:T(2,128)(2,1)} %reshape.40) | data formatting | bytes 4194304
  80.3 30.8 %all-gather.11.cloned.1.call-done = bf16[4096,256]{1,0:T(8,128)(2,1)} async-done(((bf16[512,256]{1,0:T(8,128)(2,1)}), bf16[4096,256]{1,0:T(8,128)(2,1)}) %all-gather.11.cloned.1.call-update) | async-done | bytes 2097168 | tf_op jit(solution)/shard_map/all_gather | solution.py:54
  111.1 4.0 reshape.35
  115.0 53.5 %while.15 = (s32[]{:T(128)}, f32[2,2,512]{2,1,0:T(2,128)S(1)}, f32[2,2,512]{2,1,0:T(2,128)S(1)}, f32[2,2,512,128]{3,2,1,0:T(8,128)S(1)}, bf16[2,2048,2,2,64]{1,4...) while((s32[]{:T(128)}, f32[2,2,512]{2,1,0:T(2,128)S(1)}, ...), condition=%wide.region_3.4_spmd.clone, body=%wide.region_0.3_spmd.clone.sunk | while | flops 1644963840 | bytes 65405572 | solution.py:81
  115.0 9.3 %bitcast_reduce_fusion.2 = (f32[2,2,512]{2,1,0:T(2,128)S(1)}, f32[2,2,2048,512]{3,2,1,0:T(8,128)}) fusion(bf16[512,2,2,64]{0,3,2,1:T(8,128)(2,1)S(1)} %get-tuple-element.182, bf16[2,2048,2,2,64]{1,4,3,2,0:T(8,128)(2,1)} %get-tuple-element.181, s32[]{:T(128)} %get-tuple-element.168), kind=kOutput, calls=%fused_computation.1.clone.1 | convolution fusion | flops 545257472 | bytes 18096640 | tf_op jit(solution)/shard_map/while/body/eval_jaxpr/qhmd,khmd->hmqk/dot_general | solution.py:64
  124.4 8.6 %fusion.40 = f32[2,2,512]{2,1,0:T(2,128)S(1)} fusion(f32[2,2,2048,512]{3,2,1,0:T(8,128)} %get-tuple-element.156, f32[2,2,512]{2,1,0:T(2,128)S(1)} %fusion.39), kind=kLoop, calls=%fused_computation.4.clone.1 | loop fusion | flops 12580864 | bytes 16793600 | tf_op jit(solution)/shard_map/while/body/eval_jaxpr/reduce_sum | solution.py:72
  133.9 7.9 %fusion.42 = f32[2,2,512,128]{3,2,1,0:T(8,128)S(1)} fusion(f32[2,2,2048,512]{3,2,1,0:T(8,128)} %get-tuple-element.156, f32[2,2,512]{2,1,0:T(2,128)S(1)} %fusion.39, bf16[1,2048,2,128]{3,2,1,0:T(2,128)(2,1)S(1)} %constant_dynamic-slice_fusion.2, f32[2,2,512,128]{3,2,1,0:T(8,128)S(1)} %get-tuple-element.171, f32[2,2,512]{2,1,0:T(2,128)S(1)} %get-tuple-element.158, ...), kind=kOutput, calls=%fused_computation.6.clone.1 | convolution fusion | flops 1087111168 | bytes 19939328 | tf_op jit(solution)/shard_map/while/body/eval_jaxpr/hmqk,khe->hmqe/dot_general | solution.py:73
  141.8 9.4 %bitcast_reduce_fusion.2 = (f32[2,2,512]{2,1,0:T(2,128)S(1)}, f32[2,2,2048,512]{3,2,1,0:T(8,128)}) fusion(bf16[512,2,2,64]{0,3,2,1:T(8,128)(2,1)S(1)} %get-tuple-element.182, bf16[2,2048,2,2,64]{1,4,3,2,0:T(8,128)(2,1)} %get-tuple-element.181, s32[]{:T(128)} %get-tuple-element.168), kind=kOutput, calls=%fused_computation.1.clone.1 | convolution fusion | flops 545257472 | bytes 18096640 | tf_op jit(solution)/shard_map/while/body/eval_jaxpr/qhmd,khmd->hmqk/dot_general | solution.py:64
  151.2 8.6 %fusion.40 = f32[2,2,512]{2,1,0:T(2,128)S(1)} fusion(f32[2,2,2048,512]{3,2,1,0:T(8,128)} %get-tuple-element.156, f32[2,2,512]{2,1,0:T(2,128)S(1)} %fusion.39), kind=kLoop, calls=%fused_computation.4.clone.1 | loop fusion | flops 12580864 | bytes 16793600 | tf_op jit(solution)/shard_map/while/body/eval_jaxpr/reduce_sum | solution.py:72
  160.6 7.9 %fusion.42 = f32[2,2,512,128]{3,2,1,0:T(8,128)S(1)} fusion(f32[2,2,2048,512]{3,2,1,0:T(8,128)} %get-tuple-element.156, f32[2,2,512]{2,1,0:T(2,128)S(1)} %fusion.39, bf16[1,2048,2,128]{3,2,1,0:T(2,128)(2,1)S(1)} %constant_dynamic-slice_fusion.2, f32[2,2,512,128]{3,2,1,0:T(8,128)S(1)} %get-tuple-element.171, f32[2,2,512]{2,1,0:T(2,128)S(1)} %get-tuple-element.158, ...), kind=kOutput, calls=%fused_computation.6.clone.1 | convolution fusion | flops 1087111168 | bytes 19939328 | tf_op jit(solution)/shard_map/while/body/eval_jaxpr/hmqk,khe->hmqe/dot_general | solution.py:73
  169.4 0.9 multiply_convert_fusion.1
  170.8 14.9 %all-gather.13.cloned.1.call-done = bf16[512,1024]{0,1:T(8,128)(2,1)} async-done(((bf16[512,256]{0,1:T(8,128)(2,1)}), bf16[512,1024]{0,1:T(8,128)(2,1)}) %all-gather.13.cloned.1.call-update) | async-done | bytes 1048592 | tf_op jit(solution)/shard_map/all_gather | solution.py:89
  185.7 2.0 multiply_reduce_fusion
  187.7 5.9 %psum.7 = f32[512]{0:T(512)S(1)} all-reduce(f32[512]{0:T(512)S(1)} %get-tuple-element.106), channel_id=1, replica_groups=mesh['sp'=8,'tp'=4] {'tp'}, use_global_device_ids=true, to_apply=%region_6.7 | all-reduce | flops 512 | bytes 4096 | tf_op jit(solution)/shard_map/psum | solution.py:94
  193.6 0.9 multiply_convert_fusion
  196.5 21.8 %all-gather.15.cloned.1.call-done = bf16[512,2048]{0,1:T(8,128)(2,1)} async-done(((bf16[512,512]{0,1:T(8,128)(2,1)}), bf16[512,2048]{0,1:T(8,128)(2,1)}) %all-gather.15.cloned.1.call-update) | async-done | bytes 2097168 | tf_op jit(solution)/shard_map/all_gather | solution.py:98
  218.4 94.4 %all-gather.17.cloned.1.call-done = bf16[2048,1408]{1,0:T(8,128)(2,1)} async-done(((bf16[256,1408]{1,0:T(8,128)(2,1)}), bf16[2048,1408]{1,0:T(8,128)(2,1)}) %all-gather.17.cloned.1.call-update) | async-done | bytes 5767184 | tf_op jit(solution)/shard_map/all_gather | solution.py:101
  312.7 6.7 %convolution_convert_fusion = bf16[512,1408]{1,0:T(8,128)(2,1)S(1)} fusion(bf16[512,2048]{0,1:T(8,128)(2,1)} %all-gather.15.cloned.1.call-done, bf16[2048,1408]{1,0:T(8,128)(2,1)} %all-gather.17.cloned.1.call-done), kind=kOutput, calls=%fused_computation.22 | convolution fusion | flops 2953510912 | bytes 9306112 | tf_op jit(solution)/shard_map/dot_general | solution.py:99
  320.1 3.0 collective-permute-start
  323.1 1.3 collective-permute-start.1
  324.4 1.5 slice_reduce_fusion.2
  325.9 79.5 %all-gather.21.cloned.1.call-done = bf16[11264,256]{1,0:T(8,128)(2,1)} async-done(((bf16[1408,256]{1,0:T(8,128)(2,1)}), bf16[11264,256]{1,0:T(8,128)(2,1)}) %all-gather.21.cloned.1.call-update) | async-done | bytes 5767184 | tf_op jit(solution)/shard_map/all_gather | solution.py:120
  405.3 8.3 %copy.38 = bf16[1408,8,256]{0,2,1:T(8,128)(2,1)} copy(bf16[1408,8,256]{2,0,1:T(8,128)(2,1)} %bitcast.70) | data formatting | bytes 11534336 | tf_op jit(solution)/shard_map/reshape | solution.py:120
  413.6 2.7 maximum_convert_fusion
  416.3 81.7 %all-gather.19.cloned.1.call-done = bf16[2048,1408]{1,0:T(8,128)(2,1)} async-done(((bf16[256,1408]{1,0:T(8,128)(2,1)}), bf16[2048,1408]{1,0:T(8,128)(2,1)}) %all-gather.19.cloned.1.call-update) | async-done | bytes 5767184 | tf_op jit(solution)/shard_map/all_gather | solution.py:106
  498.0 16.5 %convolution_convert_fusion.1 = bf16[512,2048]{0,1:T(8,128)(2,1)} fusion(bf16[1408,2048]{0,1:T(8,128)(2,1)} %bitcast.71, bf16[512,2048]{0,1:T(8,128)(2,1)} %all-gather.15.cloned.1.call-done, bf16[2048,1408]{1,0:T(8,128)(2,1)} %all-gather.19.cloned.1.call-done, f32[514,1408]{1,0:T(8,128)} %maximum_convert_fusion, f32[1408]{0:T(1024)} %param.26, ...), kind=kOutput, calls=%fused_computation.23 | convolution fusion | flops 5915279360 | bytes 24407040 | tf_op jit(solution)/shard_map/dot_general | solution.py:122
  514.6 29.5 %reduce-scatter.2.cloned.1.call-done = bf16[512,512]{0,1:T(8,128)(2,1)} async-done(((bf16[512,2048]{0,1:T(8,128)(2,1)}), bf16[512,512]{0,1:T(8,128)(2,1)}) %reduce-scatter.2.cloned.1.call-update) | async-done | bytes 524304 | tf_op jit(solution)/shard_map/reduce_scatter | solution.py:125
  544.1 1.2 add_convert_fusion
  545.3 1.0 copy.40
  (51 shorter events, 7.0 us)
Async XLA Ops:
  6.5 179.2 %copy-start = (bf16[1024,512]{1,0:T(8,128)(2,1)S(1)}, bf16[1024,512]{1,0:T(8,128)(2,1)}, u32[]{:S(2)}) copy-start(bf16[1024,512]{1,0:T(8,128)(2,1)} %param.21) | copy-start | bytes 3145732
  6.5 54.8 %all-gather.9.cloned.1.call-start = ((), (), s32[]{:S(2)}) async-start(), calls=%async_computation.1 | async-start | bytes 2359296 | tf_op jit(solution)/shard_map/all_gather | solution.py:53
  7.3 103.8 %all-gather.11.cloned.1.call-start = ((), (), s32[]{:S(2)}) async-start(), calls=%async_computation.2 | async-start | bytes 2359296 | tf_op jit(solution)/shard_map/all_gather | solution.py:54
  8.0 177.7 %all-gather.13.cloned.1.call-start = ((), (), s32[]{:S(2)}) async-start(), calls=%async_computation.3 | async-start | bytes 1310720 | tf_op jit(solution)/shard_map/all_gather | solution.py:89
  124.4 8.7 %copy-start.1 = (bf16[2,2048,2,128]{3,2,1,0:T(2,128)(2,1)S(1)}, bf16[2,2048,2,128]{3,2,1,0:T(2,128)(2,1)}, u32[]{:S(2)}) copy-start(bf16[2,2048,2,128]{3,2,1,0:T(2,128)(2,1)} %get-tuple-element.183) | copy-start | bytes 6291460 | tf_op jit(solution)/shard_map/while
  151.2 8.7 %copy-start.1 = (bf16[2,2048,2,128]{3,2,1,0:T(2,128)(2,1)S(1)}, bf16[2,2048,2,128]{3,2,1,0:T(2,128)(2,1)}, u32[]{:S(2)}) copy-start(bf16[2,2048,2,128]{3,2,1,0:T(2,128)(2,1)} %get-tuple-element.183) | copy-start | bytes 6291460 | tf_op jit(solution)/shard_map/while
  168.6 0.7 copy-start.4
  168.6 0.8 copy-start.5
  168.9 1.6 copy-start.2
  170.3 48.0 %all-gather.15.cloned.1.call-start = ((), (), s32[]{:S(2)}) async-start(), calls=%async_computation.4 | async-start | bytes 2621440 | tf_op jit(solution)/shard_map/all_gather | solution.py:98
  170.8 22.8 %copy-start.3 = (f32[512]{0:T(512)S(1)}, f32[512]{0:T(512)}, u32[]{:S(2)}) copy-start(f32[512]{0:T(512)} %param.22) | copy-start | bytes 6148
  194.6 118.2 %all-gather.17.cloned.1.call-start = ((), (), s32[]{:S(2)}) async-start(), calls=%async_computation.5 | async-start | bytes 6488064 | tf_op jit(solution)/shard_map/all_gather | solution.py:101
  195.2 210.2 %all-gather.21.cloned.1.call-start = ((), (), s32[]{:S(2)}) async-start(), calls=%async_computation.8 | async-start | bytes 6488064 | tf_op jit(solution)/shard_map/all_gather | solution.py:120
  195.7 302.3 %all-gather.19.cloned.1.call-start = ((), (), s32[]{:S(2)}) async-start(), calls=%async_computation.6 | async-start | bytes 6488064 | tf_op jit(solution)/shard_map/all_gather | solution.py:106
  196.5 347.6 %reduce-scatter.2.cloned.1.call-start = ((), (), s32[]{:S(2)}) async-start(), calls=%async_computation.7 | async-start | bytes 2621440 | tf_op jit(solution)/shard_map/reduce_scatter | solution.py:125
  320.1 93.6 %collective-permute-start = (bf16[1,1408]{1,0:T(2,128)(2,1)}, bf16[1,1408]{1,0:T(2,128)(2,1)}, u32[]{:S(2)}, u32[]{:S(2)}) collective-permute-start(bf16[1,1408]{1,0:T(2,128)(2,1)} %get-tuple-element.104), channel_id=1, source_target_pairs={{0,4},{4,8},{8,12},{12,16},{16,20},{20,24},{24,28},{1,5},{5,9},{9,... | collective-permute-start | bytes 8456 | tf_op jit(solution)/shard_map/ppermute | solution.py:20
  323.1 90.5 %collective-permute-start.1 = (bf16[1,1408]{1,0:T(2,128)(2,1)}, bf16[1,1408]{1,0:T(2,128)(2,1)}, u32[]{:S(2)}, u32[]{:S(2)}) collective-permute-start(bf16[1,1408]{1,0:T(2,128)(2,1)} %get-tuple-element.105), channel_id=1, source_target_pairs={{4,0},{8,4},{12,8},{16,12},{20,16},{24,20},{28,24},{5,1},{9,5},{13... | collective-permute-start | bytes 8456 | tf_op jit(solution)/shard_map/ppermute | solution.py:22
Sparse Core Ops, SparseCore 0:
  9.5 51.7 all-gather.8
  63.4 47.6 all-gather.10
  170.4 15.2 all-gather.12
  194.7 23.6 all-gather.14
  220.4 92.3 all-gather.16
  314.8 90.5 all-gather.20
  407.5 90.4 all-gather.18
  514.7 29.3 reduce-scatter.1
